TPU v7x, 32 devices: a whole 2x2x4 slice. The times are simulated.
32 devices in a mesh: ep: 8 (over z, x), tp: 4 (over y, core).
Axes of the slice: x: 2, y: 2, z: 4, core: 2. Of those that a mesh axis runs over, the one named last changes fastest.
Arguments:
- residual_in: bfloat16 [128, 2048], P('ep'), may hold values from -6 to 6
- lengths: int32 [128], P('ep'), may hold values from 1 to 511, as said below
- kv_cache: bfloat16 [128, 4, 512, 256], P('ep', 'tp'), may hold values from -640 to 640
- norm_gain_attn: float32 [2048], replicated, may hold values from 0.1 to 1.9
- query_weight: bfloat16 [2048, 2048], P(None, 'tp'), may hold values from -0.125 to 0.125
- key_weight: bfloat16 [2048, 512], P(None, 'tp'), may hold values from -0.125 to 0.125
- value_weight: bfloat16 [2048, 512], P(None, 'tp'), may hold values from -0.125 to 0.125
- diff_lambda: float32 [16], P('tp'), may hold values from 0.3 to 0.8
- head_gain: float32 [128], replicated, may hold values from 0.1 to 1.9
- out_weight: bfloat16 [2048, 2048], P(None, 'tp'), may hold values from -0.125 to 0.125
- norm_gain_ffn: float32 [2048], replicated, may hold values from 0.1 to 1.9
- route_ids: int32 [128, 2], P('ep'), may hold values from 0 to 7, as said below
- route_weights: float32 [128, 2], P('ep'), may hold values from 0.1 to 1
- expert_gate: bfloat16 [8, 2048, 512], P('ep', None, 'tp'), may hold values from -0.125 to 0.125
- expert_up: bfloat16 [8, 2048, 512], P('ep', None, 'tp'), may hold values from -0.125 to 0.125
- expert_down: bfloat16 [8, 512, 2048], P('ep', 'tp'), may hold values from -0.25 to 0.25
- dense_gate: bfloat16 [2048, 8192], P(None, 'ep'), may hold values from -0.125 to 0.125
- dense_up: bfloat16 [2048, 8192], P(None, 'ep'), may hold values from -0.125 to 0.125
- dense_down: bfloat16 [8192, 2048], P('ep'), may hold values from -0.0625 to 0.0625
- dense_mix: float32 [2048], replicated, may hold values from -0.125 to 0.125
Outputs:
- layer_out: bfloat16 [128, 2048], P('ep', 'tp')
- new_rows: bfloat16 [128, 4, 256], P('ep', 'tp')
Inputs may be any that keep to these rules, and one draw needn't show every extreme that they name: The new token stands at position lengths[b]; some sequence holds 511 positions in every draw. `route_ids`: each row names 2 different experts from one group; the groups are the 4 runs of consecutive expert numbers of equal size. Among the rows of one index of ep no expert is named more than 8 times, and some expert exactly 8 times.
All inputs are finite; a program needn't handle non-finite values.
Results may differ from a plain program's by a relative error of at most 0.008.
The roundings to bfloat16 on the way count: a program that leaves them out, or rounds other values in their place, can miss the bound.
Values may be sent and summed in bfloat16 or wider, within the bound.
A program may use at most 64 MiB of HBM per device.

v0:
```python
import jax
import jax.numpy as jnp
from jax import lax
from jax.sharding import PartitionSpec as P

QK_DIM = 64
HEAD_DIM = 128
TOPK = 2
EPS = 1e-06


def rms_rows(values, gain):
    mean_sq = jnp.mean(values * values, axis=-1, keepdims=True)
    return values * lax.rsqrt(mean_sq + EPS) * gain


def rotate(vectors, positions):
    half = vectors.shape[-1] // 2
    inverse = 10000.0 ** (-jnp.arange(half, dtype=jnp.float32) / half)
    angle = positions[:, None, None, None] * inverse
    cosine = jnp.cos(angle)
    sine = jnp.sin(angle)
    first = vectors[..., :half]
    second = vectors[..., half:]
    return jnp.concatenate(
        [first * cosine - second * sine, first * sine + second * cosine], axis=-1
    )


def normalize(scores, latest, valid):
    masked = jnp.where(valid, scores, -jnp.inf)
    top = jnp.maximum(jnp.max(masked, axis=-1), latest)
    raised = jnp.where(valid, jnp.exp(jnp.where(valid, scores, 0.0) - top[..., None]), 0.0)
    raised_new = jnp.exp(latest - top)
    total = jnp.sum(raised, axis=-1) + raised_new
    return (raised / total[..., None], raised_new / total)


def attend(query, fresh, cache, lengths, lam):
    count = fresh.shape[0]
    groups = fresh.shape[1]
    share = query.shape[1] // groups
    scale = QK_DIM ** (-0.5)
    grouped = query.reshape(count, groups, share, 2, QK_DIM)
    first = (
        jnp.einsum(
            "bgjd,bgkd->bgjk",
            grouped[:, :, :, 0],
            cache[..., :QK_DIM],
            preferred_element_type=jnp.float32,
        )
        * scale
    )
    second = (
        jnp.einsum(
            "bgjd,bgkd->bgjk",
            grouped[:, :, :, 1],
            cache[..., QK_DIM : 2 * QK_DIM],
            preferred_element_type=jnp.float32,
        )
        * scale
    )
    first_new = (
        jnp.einsum(
            "bgjd,bgd->bgj",
            grouped[:, :, :, 0],
            fresh[..., :QK_DIM],
            preferred_element_type=jnp.float32,
        )
        * scale
    )
    second_new = (
        jnp.einsum(
            "bgjd,bgd->bgj",
            grouped[:, :, :, 1],
            fresh[..., QK_DIM : 2 * QK_DIM],
            preferred_element_type=jnp.float32,
        )
        * scale
    )
    valid = (
        jnp.arange(cache.shape[2], dtype=jnp.int32)[None, None, None, :]
        < lengths[:, None, None, None]
    )
    prob_one, prob_one_new = normalize(first, first_new, valid)
    prob_two, prob_two_new = normalize(second, second_new, valid)
    weight = lam.reshape(groups, share)[None, :, :, None]
    mapped = (prob_one - weight * prob_two).astype(jnp.bfloat16)
    mapped_new = (prob_one_new - weight[..., 0] * prob_two_new).astype(jnp.bfloat16)
    output = jnp.einsum(
        "bgjk,bgkd->bgjd", mapped, cache[..., 2 * QK_DIM :], preferred_element_type=jnp.float32
    )
    output = output + mapped_new.astype(jnp.float32)[..., None] * fresh[
        :, :, None, 2 * QK_DIM :
    ].astype(jnp.float32)
    return output.reshape(count, groups * share, HEAD_DIM)


def on_device(
    residual_in,
    lengths,
    kv_cache,
    norm_gain_attn,
    query_weight,
    key_weight,
    value_weight,
    diff_lambda,
    head_gain,
    out_weight,
    norm_gain_ffn,
    route_ids,
    route_weights,
    expert_gate,
    expert_up,
    expert_down,
    dense_gate,
    dense_up,
    dense_down,
    dense_mix,
):
    seq_count, width = residual_in.shape
    lanes = lax.axis_size("tp")
    column = lax.axis_index("tp")
    quarter = width // lanes
    groups = kv_cache.shape[1]
    local_heads = diff_lambda.shape[0]
    resid = residual_in.astype(jnp.float32)
    normed = rms_rows(resid, norm_gain_attn).astype(jnp.bfloat16)
    positions = lengths.astype(jnp.float32)
    query = jnp.dot(normed, query_weight, preferred_element_type=jnp.float32).reshape(
        seq_count, local_heads, 2, QK_DIM
    )
    query = rotate(query, positions).astype(jnp.bfloat16)
    keys = jnp.dot(normed, key_weight, preferred_element_type=jnp.float32).reshape(
        seq_count, groups, 2, QK_DIM
    )
    keys = rotate(keys, positions).astype(jnp.bfloat16).reshape(seq_count, groups, 2 * QK_DIM)
    values = (
        jnp.dot(normed, value_weight, preferred_element_type=jnp.float32)
        .reshape(seq_count, groups, HEAD_DIM)
        .astype(jnp.bfloat16)
    )
    fresh = jnp.concatenate([keys, values], axis=-1)
    mixed = attend(query, fresh, kv_cache, lengths, diff_lambda)
    heads_out = (
        rms_rows(mixed, head_gain).astype(jnp.bfloat16).reshape(seq_count, local_heads * HEAD_DIM)
    )
    all_heads = lax.all_gather(heads_out, "tp", axis=1, tiled=True)
    attn_cols = jnp.dot(all_heads, out_weight, preferred_element_type=jnp.float32)
    own_cols = lax.dynamic_slice_in_dim(resid, column * quarter, quarter, 1)
    stream_cols = (own_cols + attn_cols).astype(jnp.bfloat16)
    stream = lax.all_gather(stream_cols, "tp", axis=1, tiled=True)
    ffn_in = rms_rows(stream.astype(jnp.float32), norm_gain_ffn).astype(jnp.bfloat16)
    held = expert_gate.shape[0]
    expert_total = lax.axis_size("ep") * held
    capacity = max(2, 2 * TOPK * seq_count // expert_total)
    flat_ids = route_ids.reshape(-1)
    member = (flat_ids[:, None] == jnp.arange(expert_total, dtype=jnp.int32)[None, :]).astype(
        jnp.int32
    )
    slot = jnp.sum((jnp.cumsum(member, axis=0) - member) * member, axis=1)
    target = (flat_ids * capacity + slot).reshape(seq_count, TOPK)
    picker = (
        target[None, :, :] == jnp.arange(expert_total * capacity, dtype=jnp.int32)[:, None, None]
    )
    picker = jnp.any(picker, axis=2).astype(jnp.bfloat16)
    outgoing = jnp.dot(picker, ffn_in, preferred_element_type=jnp.float32).astype(jnp.bfloat16)
    outgoing = outgoing.reshape(expert_total, capacity, ffn_in.shape[1])
    arrived = lax.all_to_all(outgoing, "ep", split_axis=0, concat_axis=0, tiled=True)
    senders = arrived.shape[0] // held
    blocked = arrived.reshape(senders, held, arrived.shape[1], width)
    gate = jnp.einsum("sjcd,jdf->sjcf", blocked, expert_gate, preferred_element_type=jnp.float32)
    upward = jnp.einsum("sjcd,jdf->sjcf", blocked, expert_up, preferred_element_type=jnp.float32)
    hidden = (jax.nn.silu(gate) * upward).astype(jnp.bfloat16)
    partial_out = jnp.einsum(
        "sjcf,jfd->sjcd", hidden, expert_down, preferred_element_type=jnp.float32
    )
    partial_out = partial_out.reshape(arrived.shape[0], arrived.shape[1], width)
    summed = lax.psum_scatter(
        partial_out.astype(jnp.bfloat16), "tp", scatter_dimension=2, tiled=True
    )
    returned = lax.all_to_all(summed, "ep", split_axis=0, concat_axis=0, tiled=True)
    flat_back = returned.reshape(expert_total * capacity, quarter)
    picked = flat_back[target]
    expert_cols = jnp.sum(route_weights[..., None] * picked.astype(jnp.float32), axis=1)
    gate_mix = jax.nn.sigmoid(jnp.sum(ffn_in.astype(jnp.float32) * dense_mix, axis=-1))
    share_rows = seq_count // lanes
    mine = lax.dynamic_slice_in_dim(ffn_in, column * share_rows, share_rows, 0)
    piece = lax.all_gather(mine, "ep", axis=0, tiled=True)
    gate = jnp.dot(piece, dense_gate, preferred_element_type=jnp.float32)
    upward = jnp.dot(piece, dense_up, preferred_element_type=jnp.float32)
    dense_hidden = (jax.nn.silu(gate) * upward).astype(jnp.bfloat16)
    dense_cols = lax.psum_scatter(
        jnp.dot(dense_hidden, dense_down, preferred_element_type=jnp.float32),
        "ep",
        scatter_dimension=0,
        tiled=True,
    )
    dense_cols = lax.all_to_all(
        dense_cols.astype(jnp.bfloat16), "tp", split_axis=1, concat_axis=0, tiled=True
    ).astype(dense_cols.dtype)
    layer_out = (
        stream_cols.astype(jnp.float32) + expert_cols + gate_mix[:, None] * dense_cols
    ).astype(jnp.bfloat16)
    return (layer_out, fresh)


def solution(mesh):
    placed = (
        P("ep", None),
        P("ep"),
        P("ep", "tp", None, None),
        P(),
        P(None, "tp"),
        P(None, "tp"),
        P(None, "tp"),
        P("tp"),
        P(),
        P(None, "tp"),
        P(),
        P("ep", None),
        P("ep", None),
        P("ep", None, "tp"),
        P("ep", None, "tp"),
        P("ep", "tp", None),
        P(None, "ep"),
        P(None, "ep"),
        P("ep", None),
        P(),
    )
    return jax.shard_map(
        on_device,
        mesh=mesh,
        in_specs=placed,
        out_specs=(P("ep", "tp"), P("ep", "tp", None)),
        check_vma=False,
    )
```

profile of v0, /device:TPU:0, one launch (start us, length us, event | category | flops | bytes accessed | tf_op | source)
XLA Modules:
  0.0 165.9 jit_solution(6346756929134641032)
XLA Ops:
  7.2 0.8 convert_element_type.109
  8.0 0.7 iota_compare_fusion
  8.7 1.0 multiply_reduce_fusion.1
  9.7 0.9 convert_element_type.107
  10.6 1.3 fusion.73
  11.9 1.3 fusion.70
  13.2 0.1 reshape.337
  13.3 0.1 fusion.72
  13.5 1.3 fusion.69
  14.9 0.1 multiply_cosine_fusion
  15.0 0.1 subtract_convert_fusion.1
  15.1 0.1 pad_maximum_fusion.1
  15.2 0.1 convert_element_type.110
  15.4 0.1 fusion.55
  15.5 0.1 fusion.59
  15.6 2.5 %fusion.11 = f32[16,4,512]{2,1,0:T(4,128)S(1)} fusion(bf16[16,4,64]{2,1,0:T(4,128)(2,1)S(1)} %get-tuple-element.12, bf16[16,1,512,256]{3,2,1,0:T(8,128)(2,1)} %param.22), kind=kOutput, calls=%fused_computation.14 | convolution fusion | flops 4227072 | bytes 2236416 | tf_op jit(solution)/shard_map/bgjd,bgkd->bgjk/dot_general | solution.py:55
  18.2 0.1 fusion.61
  18.3 2.3 %select_reduce_fusion.1 = (f32[16,4]{1,0:T(8,128)S(1)}, f32[16,4]{1,0:T(8,128)S(1)}, f32[16,4,512]{2,1,0:T(4,128)S(1)}) fusion(pred[16,512]{1,0:T(8,128)(4,1)S(1)} %iota_compare_fusion, f32[16,4,512]{2,1,0:T(4,128)S(1)} %fusion.11, bf16[16,4,64]{2,1,0:T(4,128)(2,1)S(1)} %get-tuple-element.13, bf16[16,1,512,256]{3,2,1,0:T(8,128)(2,1)} %param.22), kind=kOutput, calls=%fused_computation.44 | convolution fusion | flops 4358016 | bytes 2376192 | tf_op jit(solution)/shard_map/bgjd,bgkd->bgjk/dot_general | solution.py:46
  20.7 0.3 fusion.34
  21.0 0.6 multiply_reduce_fusion.3
  21.7 6.2 %all_gather.9 = bf16[16,2048]{1,0:T(8,128)(2,1)S(1)} all-gather(bf16[16,512]{1,0:T(8,128)(2,1)S(1)} %fusion.45), channel_id=1, replica_groups=mesh['ep'=8,'tp'=4] {'tp'}, dimensions={1}, use_global_device_ids=true | all-gather | bytes 81920 | tf_op jit(solution)/shard_map/all_gather | solution.py:148
  28.0 2.0 %fusion.18 = bf16[16,512]{1,0:T(8,128)(2,1)S(1)} fusion(bf16[16,2048]{1,0:T(8,128)(2,1)S(1)} %all_gather.9, bf16[2048,512]{1,0:T(8,128)(2,1)} %param.29, f32[16,2048]{1,0:T(8,128)S(1)} %convert_element_type.107, s32[]{:T(128)S(6)} %select_n.34), kind=kOutput, calls=%fused_computation.22 | convolution fusion | flops 33570816 | bytes 2211844 | tf_op jit(solution)/shard_map/dot_general | solution.py:149
  29.9 5.5 %all_gather.10 = bf16[16,2048]{1,0:T(8,128)(2,1)S(1)} all-gather(bf16[16,512]{1,0:T(8,128)(2,1)S(1)} %fusion.18), channel_id=1, replica_groups=mesh['ep'=8,'tp'=4] {'tp'}, dimensions={1}, use_global_device_ids=true | all-gather | bytes 81920 | tf_op jit(solution)/shard_map/all_gather | solution.py:152
  35.5 0.1 fusion.25
  35.7 0.1 eq.28
  35.9 0.2 select_reduce_fusion.2
  36.2 0.1 copy.70
  36.4 0.2 multiply_reduce_fusion
  36.6 1.0 fusion
  37.6 6.0 %all-to-all-start = ((bf16[8,8,2048]{2,1,0:T(8,128)(2,1)}), bf16[8,8,2048]{2,1,0:T(8,128)(2,1)S(1)}, u32[]{:S(2)}, u32[]{:S(2)}) async-start(bf16[8,8,2048]{2,1,0:T(8,128)(2,1)} %fusion), calls=%async_computation | async-start | bytes 524288 | tf_op jit(solution)/shard_map/all_to_all | solution.py:169
  43.6 33.4 %all-gather = bf16[8,4,2048]{2,1,0:T(4,128)(2,1)S(1)} all-gather(bf16[1,4,2048]{2,1,0:T(4,128)(2,1)S(1)} %dynamic-slice_bitcast_fusion), channel_id=1, replica_groups=mesh['ep'=8,'tp'=4] {'ep'}, dimensions={0}, use_global_device_ids=true | all-gather | bytes 147456 | tf_op jit(solution)/shard_map/all_gather | solution.py:189
  77.1 3.0 %fusion.74 = f32[32,1024]{1,0:T(8,128)S(1)} fusion(bf16[32,2048]{1,0:T(8,128)(2,1)S(1)} %reshape.365, bf16[2048,1024]{1,0:T(8,128)(2,1)} %param.36), kind=kOutput, calls=%fused_computation.125 | convolution fusion | flops 134217728 | bytes 4456448 | tf_op jit(solution)/shard_map/dot_general | solution.py:190
  80.1 5.1 %fusion.15 = f32[32,2048]{1,0:T(8,128)S(1)} fusion(bf16[1024,2048]{1,0:T(8,128)(2,1)} %param.38, bf16[32,2048]{1,0:T(8,128)(2,1)S(1)} %reshape.365, bf16[2048,1024]{1,0:T(8,128)(2,1)} %param.37, f32[32,1024]{1,0:T(8,128)S(1)} %fusion.74), kind=kOutput, calls=%fused_computation.16 | convolution fusion | flops 268632064 | bytes 8912896 | tf_op jit(solution)/shard_map/dot_general | solution.py:194
  85.2 0.6 dynamic-slice
  86.4 37.8 %all-reduce.2 = bf16[32,2048]{1,0:T(8,128)(2,1)S(1)} all-reduce(f32[32,2048]{1,0:T(8,128)S(1)} %fusion.15), channel_id=3, replica_groups=mesh['ep'=8,'tp'=4] {'ep'}, use_global_device_ids=true, to_apply=%region_13.14.clone | all-reduce | flops 65536 | bytes 393216
  124.2 1.3 convolution_bitcast_fusion.1
  125.5 2.1 %convolution_convert_fusion = bf16[8,8,2048]{2,1,0:T(8,128)(2,1)} fusion(bf16[8,8,2048]{2,1,0:T(8,128)(2,1)S(1)} %all-to-all-done, bf16[1,128,2048]{2,1,0:T(8,128)(2,1)S(1)} %copy-done.2, bf16[1,2048,128]{2,1,0:T(8,128)(2,1)} %param.34, f32[8,1,8,128]{3,2,0,1:T(8,128)S(1)} %convolution_bitcast_fusion.1), kind=kOutput, calls=%fused_computation.1 | convolution fusion | flops 67289088 | bytes 1605632 | tf_op jit(solution)/shard_map/sjcf,jfd->sjcd/dot_general | solution.py:175
  127.6 0.6 dynamic-slice_convert_fusion
  128.3 3.3 %all-to-all-start.2 = ((bf16[4,4,512]{2,0,1:T(4,128)(2,1)}), bf16[4,4,512]{2,0,1:T(4,128)(2,1)S(1)}, u32[]{:S(2)}, u32[]{:S(2)}) async-start(bf16[4,4,512]{2,0,1:T(4,128)(2,1)} %bitcast.35), calls=%async_computation.3 | async-start | bytes 32768 | tf_op jit(solution)/shard_map/all_to_all | solution.py:199
  131.6 0.1 reshape.355
  131.7 0.6 pad_maximum_fusion.2
  132.4 2.9 %all-to-all-done.2 = bf16[4,4,512]{2,0,1:T(4,128)(2,1)S(1)} async-done(((bf16[4,4,512]{2,0,1:T(4,128)(2,1)}), bf16[4,4,512]{2,0,1:T(4,128)(2,1)S(1)}, u32[]{:S(2)}, u32[]{:S(2)}) %all-to-all-start.2) | async-done | bytes 16416 | tf_op jit(solution)/shard_map/all_to_all | solution.py:199
  135.4 9.8 %reduce-scatter.2.cloned.1.call-done = bf16[8,8,512]{2,1,0:T(8,128)(2,1)} async-done(((bf16[8,8,2048]{2,1,0:T(8,128)(2,1)}), bf16[8,8,512]{2,1,0:T(8,128)(2,1)}) %reduce-scatter.2.cloned.1.call-update) | async-done | bytes 65552 | tf_op jit(solution)/shard_map/reduce_scatter | solution.py:179
  145.2 5.5 %all-to-all-start.1 = ((bf16[8,8,512]{2,1,0:T(8,128)(2,1)}), bf16[8,8,512]{2,1,0:T(8,128)(2,1)S(1)}, u32[]{:S(2)}, u32[]{:S(2)}) async-start(bf16[8,8,512]{2,1,0:T(8,128)(2,1)} %reduce-scatter.2.cloned.1.call-done), calls=%async_computation.2 | async-start | bytes 131072 | tf_op jit(solution)/shard_map/all_to_all | solution.py:182
  150.7 6.9 %all-to-all-done.1 = bf16[8,8,512]{2,1,0:T(8,128)(2,1)S(1)} async-done(((bf16[8,8,512]{2,1,0:T(8,128)(2,1)}), bf16[8,8,512]{2,1,0:T(8,128)(2,1)S(1)}, u32[]{:S(2)}, u32[]{:S(2)}) %all-to-all-start.1) | async-done | bytes 65568 | tf_op jit(solution)/shard_map/all_to_all | solution.py:182
  157.6 0.6 gather_fusion
  158.2 0.1 multiply_reduce_fusion.2
  158.4 0.7 add_convert_fusion.1
  (50 shorter events, 1.2 us)
Async XLA Ops:
  7.2 4.7 %copy-start = (bf16[2048,512]{1,0:T(8,128)(2,1)S(1)}, bf16[2048,512]{1,0:T(8,128)(2,1)}, u32[]{:S(2)}) copy-start(bf16[2048,512]{1,0:T(8,128)(2,1)} %param.24) | copy-start | bytes 6291460
  11.9 9.1 %copy-start.7 = (f32[4]{0:T(128)S(1)}, f32[4]{0:T(128)}, u32[]{:S(2)}) copy-start(f32[4]{0:T(128)} %param.27) | copy-start | bytes 52
  15.3 5.7 %copy-start.1 = (bf16[16,1,512,256]{3,2,1,0:T(8,128)(2,1)S(1)}, bf16[16,1,512,256]{3,2,1,0:T(8,128)(2,1)}, u32[]{:S(2)}) copy-start(bf16[16,1,512,256]{3,2,1,0:T(8,128)(2,1)} %param.22) | copy-start | bytes 12582916
  18.2 3.5 %copy-start.8 = (f32[128]{0:T(128)S(1)}, f32[128]{0:T(128)}, u32[]{:S(2)}) copy-start(f32[128]{0:T(128)} %param.28) | copy-start | bytes 1540
  20.6 15.0 %copy-start.5 = (s32[16,2]{0,1:T(2,128)S(1)}, s32[16,2]{0,1:T(2,128)}, u32[]{:S(2)}) copy-start(s32[16,2]{0,1:T(2,128)} %param.31) | copy-start | bytes 388
  20.6 15.7 %copy-start.3 = (f32[2048]{0:T(1024)S(1)}, f32[2048]{0:T(1024)}, u32[]{:S(2)}) copy-start(f32[2048]{0:T(1024)} %param.39) | copy-start | bytes 24580
  20.6 15.7 %copy-start.4 = (f32[2048]{0:T(1024)S(1)}, f32[2048]{0:T(1024)}, u32[]{:S(2)}) copy-start(f32[2048]{0:T(1024)} %param.30) | copy-start | bytes 24580
  37.6 86.6 %all-to-all-start = ((bf16[8,8,2048]{2,1,0:T(8,128)(2,1)}), bf16[8,8,2048]{2,1,0:T(8,128)(2,1)S(1)}, u32[]{:S(2)}, u32[]{:S(2)}) async-start(bf16[8,8,2048]{2,1,0:T(8,128)(2,1)} %fusion), calls=%async_computation | async-start | bytes 524288 | tf_op jit(solution)/shard_map/all_to_all | solution.py:169
  43.5 101.6 %reduce-scatter.2.cloned.1.call-start = ((), (), s32[]{:S(2)}) async-start(), calls=%async_computation.4 | async-start | bytes 327680 | tf_op jit(solution)/shard_map/reduce_scatter | solution.py:179
  80.1 5.1 %copy-start.9 = (u32[32]{0:T(128)S(1)}, u32[32]{0:T(128)}, u32[]{:S(2)}) copy-start(u32[32]{0:T(128)} %constant.59) | copy-start | bytes 388
  80.1 45.4 %copy-start.2 = (bf16[1,128,2048]{2,1,0:T(8,128)(2,1)S(1)}, bf16[1,128,2048]{2,1,0:T(8,128)(2,1)}, u32[]{:S(2)}) copy-start(bf16[1,128,2048]{2,1,0:T(8,128)(2,1)} %param.35) | copy-start | bytes 1572868
  80.1 52.2 %copy-start.6 = (f32[16,2]{0,1:T(2,128)S(1)}, f32[16,2]{0,1:T(2,128)}, u32[]{:S(2)}) copy-start(f32[16,2]{0,1:T(2,128)} %param.32) | copy-start | bytes 388
  128.3 7.1 %all-to-all-start.2 = ((bf16[4,4,512]{2,0,1:T(4,128)(2,1)}), bf16[4,4,512]{2,0,1:T(4,128)(2,1)S(1)}, u32[]{:S(2)}, u32[]{:S(2)}) async-start(bf16[4,4,512]{2,0,1:T(4,128)(2,1)} %bitcast.35), calls=%async_computation.3 | async-start | bytes 32768 | tf_op jit(solution)/shard_map/all_to_all | solution.py:199
  145.2 12.4 %all-to-all-start.1 = ((bf16[8,8,512]{2,1,0:T(8,128)(2,1)}), bf16[8,8,512]{2,1,0:T(8,128)(2,1)S(1)}, u32[]{:S(2)}, u32[]{:S(2)}) async-start(bf16[8,8,512]{2,1,0:T(8,128)(2,1)} %reduce-scatter.2.cloned.1.call-done), calls=%async_computation.2 | async-start | bytes 131072 | tf_op jit(solution)/shard_map/all_to_all | solution.py:182
Sparse Core Ops, SparseCore 0:
  127.8 17.3 reduce-scatter.1
where the time goes:
time: 167 us; the launch traced here: 166 us
  blocking collectives  82.9 us (50%)
  matrix products  24.1 us (14%)
  waiting for transfers between devices  19.6 us (12%)
  between operations  15 us (9%)
  starting transfers between devices  14.8 us (9%)
  other arithmetic  6.43 us (4%)
  local copies, waits for them, and re-layouts  3.1 us (2%)
    unnamed x1, blocking collectives  37.8 us
    all_gather x1, blocking collectives, on_device(): piece = lax.all_gather(mine, 'ep', axis=0, tiled=True)  33.4 us
    reduce_scatter x1, waiting for transfers between devices, on_device(): lax.psum_scatter(partial_out.astype(jnp.bfloat16), 'tp', scatter_dimensio...  9.79 us
    all_to_all x1, waiting for transfers between devices, on_device(): lax.all_to_all(summed, 'ep', split_axis=0, concat_axis=0, tiled=True)  6.88 us
    all_gather x1, blocking collectives, on_device(): all_heads = lax.all_gather(heads_out, 'tp', axis=1, tiled=True)  6.24 us
    all_to_all x1, starting transfers between devices, on_device(): lax.all_to_all(outgoing, 'ep', split_axis=0, concat_axis=0, tiled=True)  5.98 us
    all_gather x1, blocking collectives, on_device(): stream = lax.all_gather(stream_cols, 'tp', axis=1, tiled=True)  5.52 us
    all_to_all x1, starting transfers between devices, on_device(): lax.all_to_all(summed, 'ep', split_axis=0, concat_axis=0, tiled=True)  5.5 us
  transfers between devices with their start and end apart: 4, of which 3 were waited for; matrix products, arithmetic and copies ran while one was open for 6% of the time, Pallas kernels for 0%

commit v1 on v0

--- a/solution.py
+++ b/solution.py
@@ -186,7 +186,14 @@
     gate_mix = jax.nn.sigmoid(jnp.sum(ffn_in.astype(jnp.float32) * dense_mix, axis=-1))
     share_rows = seq_count // lanes
     mine = lax.dynamic_slice_in_dim(ffn_in, column * share_rows, share_rows, 0)
-    piece = lax.all_gather(mine, "ep", axis=0, tiled=True)
+    size = lax.axis_size("ep")
+    right = [(i, (i + 1) % size) for i in range(size)]
+    terms = [mine]
+    for far in range(1, size):
+        terms = [lax.ppermute(terms[0], "ep", right), *terms]
+    whole = jnp.concatenate(terms, axis=0)
+    shift = (lax.axis_index("ep") + 1) * terms[-1].shape[0]
+    piece = jnp.roll(whole, shift, axis=0)
     gate = jnp.dot(piece, dense_gate, preferred_element_type=jnp.float32)
     upward = jnp.dot(piece, dense_up, preferred_element_type=jnp.float32)
     dense_hidden = (jax.nn.silu(gate) * upward).astype(jnp.bfloat16)

time: 167 us -> 159 us (0.952)
  blocking collectives: 82.9 us -> 47.9 us
  waiting for transfers between devices: 19.6 us -> 45.2 us
  starting transfers between devices: 14.8 us -> 16.9 us
    ppermute x0 -> x7, waiting for transfers between devices: none -> 34.6 us  [on_device(): terms = [lax.ppermute(terms[0], 'ep', right), *terms]]
    all_gather x1 -> x0, blocking collectives: 33.4 us -> none  [on_device(): piece = lax.all_gather(mine, 'ep', axis=0, tiled=True)]
    reduce_scatter x1, waiting for transfers between devices: 9.79 us -> 0.01 us  [on_device(): lax.psum_scatter(partial_out.astype(jnp.bfloat16), 'tp', scatter_dimensio...]
    ppermute x0 -> x7, starting transfers between devices: none -> 3.77 us  [on_device(): terms = [lax.ppermute(terms[0], 'ep', right), *terms]]
  transfers between devices with their start and end apart: 4 -> 11, of which waited for: 3 -> 8; matrix products, arithmetic and copies ran while one was open for 6% -> 8% of each run, Pallas kernels for 0% -> 0%
where the time goes in v1:
time: 159 us; the launch traced here: 158 us
  blocking collectives  47.9 us (30%)
  waiting for transfers between devices  45.2 us (28%)
  matrix products  23 us (14%)
  starting transfers between devices  16.9 us (11%)
  between operations  15.1 us (9%)
  other arithmetic  6.42 us (4%)
  local copies, waits for them, and re-layouts  3.32 us (2%)
    unnamed x1, blocking collectives  36.2 us
    ppermute x7, waiting for transfers between devices, on_device(): terms = [lax.ppermute(terms[0], 'ep', right), *terms]  34.6 us
    all_to_all x1, waiting for transfers between devices, on_device(): lax.all_to_all(summed, 'ep', split_axis=0, concat_axis=0, tiled=True)  6.88 us
    all_gather x1, blocking collectives, on_device(): all_heads = lax.all_gather(heads_out, 'tp', axis=1, tiled=True)  6.24 us
    all_to_all x1, starting transfers between devices, on_device(): lax.all_to_all(outgoing, 'ep', split_axis=0, concat_axis=0, tiled=True)  6 us
    all_gather x1, blocking collectives, on_device(): stream = lax.all_gather(stream_cols, 'tp', axis=1, tiled=True)  5.52 us
    dot_general x1, matrix products, on_device(): jnp.dot(dense_hidden, dense_down, preferred_element_type=jnp.float32)  5.07 us
    all_to_all x1, starting transfers between devices, on_device(): lax.all_to_all(summed, 'ep', split_axis=0, concat_axis=0, tiled=True)  3.84 us
  transfers between devices with their start and end apart: 11, of which 8 were waited for; matrix products, arithmetic and copies ran while one was open for 8% of the time, Pallas kernels for 0%

profile of v1, /device:TPU:0, one launch (start us, length us, event | category | flops | bytes accessed | tf_op | source)
XLA Modules:
  0.0 157.8 jit_solution(13260649364960444226)
XLA Ops:
  7.2 0.8 convert_element_type.109
  8.0 0.7 iota_compare_fusion
  8.8 1.0 multiply_reduce_fusion.1
  9.7 0.9 convert_element_type.107
  10.6 1.3 fusion.75
  11.9 0.1 reshape.337
  12.0 0.1 fusion.77
  12.2 1.3 fusion.74
  13.6 0.1 multiply_cosine_fusion
  14.2 2.5 %fusion.11 = f32[16,4,512]{2,1,0:T(4,128)S(1)} fusion(bf16[16,4,64]{2,1,0:T(4,128)(2,1)S(1)} %get-tuple-element.12, bf16[16,1,512,256]{3,2,1,0:T(8,128)(2,1)} %param.22), kind=kOutput, calls=%fused_computation.13 | convolution fusion | flops 4227072 | bytes 2236416 | tf_op jit(solution)/shard_map/bgjd,bgkd->bgjk/dot_general | solution.py:55
  16.7 0.1 fusion.61
  16.9 0.2 fusion.78
  17.1 0.1 fusion.63
  17.2 2.3 %select_reduce_fusion.1 = (f32[16,4]{1,0:T(8,128)S(1)}, f32[16,4]{1,0:T(8,128)S(1)}, f32[16,4,512]{2,1,0:T(4,128)S(1)}) fusion(pred[16,512]{1,0:T(8,128)(4,1)S(1)} %iota_compare_fusion, f32[16,4,512]{2,1,0:T(4,128)S(1)} %fusion.11, bf16[16,4,64]{2,1,0:T(4,128)(2,1)S(1)} %get-tuple-element.13, bf16[16,1,512,256]{3,2,1,0:T(8,128)(2,1)} %param.22), kind=kOutput, calls=%fused_computation.37 | convolution fusion | flops 4358016 | bytes 2376192 | tf_op jit(solution)/shard_map/bgjd,bgkd->bgjk/dot_general | solution.py:46
  19.6 0.3 fusion.36
  20.0 0.6 multiply_reduce_fusion.3
  20.7 6.2 %all_gather.6 = bf16[16,2048]{1,0:T(8,128)(2,1)S(1)} all-gather(bf16[16,512]{1,0:T(8,128)(2,1)S(1)} %fusion.47), channel_id=1, replica_groups=mesh['ep'=8,'tp'=4] {'tp'}, dimensions={1}, use_global_device_ids=true | all-gather | bytes 81920 | tf_op jit(solution)/shard_map/all_gather | solution.py:148
  26.9 2.0 %fusion.16 = bf16[16,512]{1,0:T(8,128)(2,1)S(1)} fusion(bf16[16,2048]{1,0:T(8,128)(2,1)S(1)} %all_gather.6, bf16[2048,512]{1,0:T(8,128)(2,1)} %param.29, f32[16,2048]{1,0:T(8,128)S(1)} %convert_element_type.107, s32[]{:T(128)S(6)} %select_n.47), kind=kOutput, calls=%fused_computation.19 | convolution fusion | flops 33570816 | bytes 2211844 | tf_op jit(solution)/shard_map/dot_general | solution.py:149
  29.0 5.5 %all_gather.7 = bf16[16,2048]{1,0:T(8,128)(2,1)S(1)} all-gather(bf16[16,512]{1,0:T(8,128)(2,1)S(1)} %fusion.16), channel_id=1, replica_groups=mesh['ep'=8,'tp'=4] {'tp'}, dimensions={1}, use_global_device_ids=true | all-gather | bytes 81920 | tf_op jit(solution)/shard_map/all_gather | solution.py:152
  34.5 0.1 fusion.23
  34.6 0.2 multiply_reduce_fusion
  34.9 1.7 %collective-permute-start = (bf16[4,2048]{1,0:T(4,128)(2,1)S(1)}, bf16[4,2048]{1,0:T(4,128)(2,1)S(1)}, u32[]{:S(2)}, u32[]{:S(2)}) collective-permute-start(bf16[4,2048]{1,0:T(4,128)(2,1)S(1)} %constant_dynamic-slice_fusion), channel_id=1, source_target_pairs={{0,4},{4,8},{8,12},{12,16},{16,20},{20,24},{24,28},{28,0},{1,5},{5... | collective-permute-start | bytes 49160 | tf_op jit(solution)/shard_map/ppermute | solution.py:193
  36.9 4.5 %collective-permute-done = bf16[4,2048]{1,0:T(4,128)(2,1)S(1)} collective-permute-done((bf16[4,2048]{1,0:T(4,128)(2,1)S(1)}, bf16[4,2048]{1,0:T(4,128)(2,1)S(1)}, u32[]{:S(2)}, u32[]{:S(2)}) %collective-permute-start) | collective-permute-done | bytes 16416 | tf_op jit(solution)/shard_map/ppermute | solution.py:193
  41.4 0.2 select_reduce_fusion.2
  41.7 6.1 %collective-permute-done.1 = bf16[4,2048]{1,0:T(4,128)(2,1)S(1)} collective-permute-done((bf16[4,2048]{1,0:T(4,128)(2,1)S(1)}, bf16[4,2048]{1,0:T(4,128)(2,1)S(1)}, u32[]{:S(2)}, u32[]{:S(2)}) %collective-permute-start.1) | collective-permute-done | bytes 16416 | tf_op jit(solution)/shard_map/ppermute | solution.py:193
  47.8 6.4 %collective-permute-done.2 = bf16[4,2048]{1,0:T(4,128)(2,1)S(1)} collective-permute-done((bf16[4,2048]{1,0:T(4,128)(2,1)S(1)}, bf16[4,2048]{1,0:T(4,128)(2,1)S(1)}, u32[]{:S(2)}, u32[]{:S(2)}) %collective-permute-start.2) | collective-permute-done | bytes 16416 | tf_op jit(solution)/shard_map/ppermute | solution.py:193
  54.3 6.4 %collective-permute-done.3 = bf16[4,2048]{1,0:T(4,128)(2,1)S(1)} collective-permute-done((bf16[4,2048]{1,0:T(4,128)(2,1)S(1)}, bf16[4,2048]{1,0:T(4,128)(2,1)S(1)}, u32[]{:S(2)}, u32[]{:S(2)}) %collective-permute-start.3) | collective-permute-done | bytes 16416 | tf_op jit(solution)/shard_map/ppermute | solution.py:193
  60.7 1.0 fusion
  61.6 6.0 %all-to-all-start = ((bf16[8,8,2048]{2,1,0:T(8,128)(2,1)}), bf16[8,8,2048]{2,1,0:T(8,128)(2,1)S(1)}, u32[]{:S(2)}, u32[]{:S(2)}) async-start(bf16[8,8,2048]{2,1,0:T(8,128)(2,1)} %fusion), calls=%async_computation | async-start | bytes 524288 | tf_op jit(solution)/shard_map/all_to_all | solution.py:169
  67.7 2.0 %collective-permute-start.5 = (bf16[4,2048]{1,0:T(4,128)(2,1)S(1)}, bf16[4,2048]{1,0:T(4,128)(2,1)S(1)}, u32[]{:S(2)}, u32[]{:S(2)}) collective-permute-start(bf16[4,2048]{1,0:T(4,128)(2,1)S(1)} %collective-permute-done.4), channel_id=1, source_target_pairs={{0,4},{4,8},{8,12},{12,16},{16,20},{20,24},{24,28},{28,0},{1,5},{5... | collective-permute-start | bytes 49160 | tf_op jit(solution)/shard_map/ppermute | solution.py:193
  69.7 6.8 %collective-permute-done.5 = bf16[4,2048]{1,0:T(4,128)(2,1)S(1)} collective-permute-done((bf16[4,2048]{1,0:T(4,128)(2,1)S(1)}, bf16[4,2048]{1,0:T(4,128)(2,1)S(1)}, u32[]{:S(2)}, u32[]{:S(2)}) %collective-permute-start.5) | collective-permute-done | bytes 16416 | tf_op jit(solution)/shard_map/ppermute | solution.py:193
  76.6 0.6 pad_maximum_fusion.2
  77.4 0.6 dynamic-slice
  78.6 4.4 %collective-permute-done.6 = bf16[4,2048]{1,0:T(4,128)(2,1)S(1)} collective-permute-done((bf16[4,2048]{1,0:T(4,128)(2,1)S(1)}, bf16[4,2048]{1,0:T(4,128)(2,1)S(1)}, u32[]{:S(2)}, u32[]{:S(2)}) %collective-permute-start.6) | collective-permute-done | bytes 16416 | tf_op jit(solution)/shard_map/ppermute | solution.py:193
  83.0 0.3 concatenate.34
  83.3 3.0 %fusion.29 = f32[32,1024]{1,0:T(8,128)S(1)} fusion(bf16[2048,1024]{1,0:T(8,128)(2,1)} %param.36, bf16[64,2048]{1,0:T(8,128)(2,1)S(1)} %concatenate.34, s32[]{:T(128)S(6)} %select_n.57), kind=kOutput, calls=%fused_computation.43 | convolution fusion | flops 134217728 | bytes 4456452 | tf_op jit(solution)/shard_map/dot_general | solution.py:197
  86.3 1.3 convolution_bitcast_fusion.1
  87.6 2.1 %convolution_convert_fusion = bf16[8,8,2048]{2,1,0:T(8,128)(2,1)} fusion(bf16[8,8,2048]{2,1,0:T(8,128)(2,1)S(1)} %all-to-all-done, bf16[1,128,2048]{2,1,0:T(8,128)(2,1)S(1)} %copy-done.3, bf16[1,2048,128]{2,1,0:T(8,128)(2,1)} %param.34, f32[8,1,8,128]{3,2,0,1:T(8,128)S(1)} %convolution_bitcast_fusion.1), kind=kOutput, calls=%fused_computation.1 | convolution fusion | flops 67289088 | bytes 1605632 | tf_op jit(solution)/shard_map/sjcf,jfd->sjcd/dot_general | solution.py:175
  89.7 5.1 %fusion.34 = f32[32,2048]{1,0:T(8,128)S(1)} fusion(bf16[1024,2048]{1,0:T(8,128)(2,1)} %param.38, f32[32,1024]{1,0:T(8,128)S(1)} %fusion.29, bf16[2048,1024]{1,0:T(8,128)(2,1)} %param.37, bf16[64,2048]{1,0:T(8,128)(2,1)S(1)} %concatenate.34, s32[]{:T(128)S(6)} %select_n.57), kind=kOutput, calls=%fused_computation.45 | convolution fusion | flops 268632064 | bytes 8912900 | tf_op jit(solution)/shard_map/dot_general | solution.py:201
  94.8 36.2 %all-reduce.2 = bf16[32,2048]{1,0:T(8,128)(2,1)S(1)} all-reduce(f32[32,2048]{1,0:T(8,128)S(1)} %fusion.34), channel_id=3, replica_groups=mesh['ep'=8,'tp'=4] {'ep'}, use_global_device_ids=true, to_apply=%region_13.14.clone | all-reduce | flops 65536 | bytes 393216
  131.0 0.6 dynamic-slice_convert_fusion
  131.6 3.3 %all-to-all-start.2 = ((bf16[4,4,512]{2,0,1:T(4,128)(2,1)}), bf16[4,4,512]{2,0,1:T(4,128)(2,1)S(1)}, u32[]{:S(2)}, u32[]{:S(2)}) async-start(bf16[4,4,512]{2,0,1:T(4,128)(2,1)} %bitcast.34), calls=%async_computation.3 | async-start | bytes 32768 | tf_op jit(solution)/shard_map/all_to_all | solution.py:206
  135.0 3.7 %all-to-all-done.2 = bf16[4,4,512]{2,0,1:T(4,128)(2,1)S(1)} async-done(((bf16[4,4,512]{2,0,1:T(4,128)(2,1)}), bf16[4,4,512]{2,0,1:T(4,128)(2,1)S(1)}, u32[]{:S(2)}, u32[]{:S(2)}) %all-to-all-start.2) | async-done | bytes 16416 | tf_op jit(solution)/shard_map/all_to_all | solution.py:206
  138.7 3.8 %all-to-all-start.1 = ((bf16[8,8,512]{2,1,0:T(8,128)(2,1)}), bf16[8,8,512]{2,1,0:T(8,128)(2,1)S(1)}, u32[]{:S(2)}, u32[]{:S(2)}) async-start(bf16[8,8,512]{2,1,0:T(8,128)(2,1)} %reduce-scatter.2.cloned.1.call-done), calls=%async_computation.2 | async-start | bytes 131072 | tf_op jit(solution)/shard_map/all_to_all | solution.py:182
  142.6 6.9 %all-to-all-done.1 = bf16[8,8,512]{2,1,0:T(8,128)(2,1)S(1)} async-done(((bf16[8,8,512]{2,1,0:T(8,128)(2,1)}), bf16[8,8,512]{2,1,0:T(8,128)(2,1)S(1)}, u32[]{:S(2)}, u32[]{:S(2)}) %all-to-all-start.1) | async-done | bytes 65568 | tf_op jit(solution)/shard_map/all_to_all | solution.py:182
  149.4 0.6 gather_fusion
  150.1 0.1 multiply_reduce_fusion.2
  150.3 0.7 add_convert_fusion.1
  (69 shorter events, 1.7 us)
Async XLA Ops:
  7.2 3.4 %copy-start = (bf16[2048,512]{1,0:T(8,128)(2,1)S(1)}, bf16[2048,512]{1,0:T(8,128)(2,1)}, u32[]{:S(2)}) copy-start(bf16[2048,512]{1,0:T(8,128)(2,1)} %param.24) | copy-start | bytes 6291460
  7.2 9.6 %copy-start.1 = (bf16[16,2048]{1,0:T(8,128)(2,1)S(1)}, bf16[16,2048]{1,0:T(8,128)(2,1)}, u32[]{:S(2)}) copy-start(bf16[16,2048]{1,0:T(8,128)(2,1)} %param.20) | copy-start | bytes 196612
  7.2 9.6 %copy-start.5 = (f32[2048]{0:T(1024)S(1)}, f32[2048]{0:T(1024)}, u32[]{:S(2)}) copy-start(f32[2048]{0:T(1024)} %param.23) | copy-start | bytes 24580
  7.2 9.6 %copy-start.4 = (bf16[2048,128]{1,0:T(8,128)(2,1)S(1)}, bf16[2048,128]{1,0:T(8,128)(2,1)}, u32[]{:S(2)}) copy-start(bf16[2048,128]{1,0:T(8,128)(2,1)} %param.26) | copy-start | bytes 1572868
  10.6 9.3 %copy-start.10 = (f32[4]{0:T(128)S(1)}, f32[4]{0:T(128)}, u32[]{:S(2)}) copy-start(f32[4]{0:T(128)} %param.27) | copy-start | bytes 52
  14.0 6.0 %copy-start.2 = (bf16[16,1,512,256]{3,2,1,0:T(8,128)(2,1)S(1)}, bf16[16,1,512,256]{3,2,1,0:T(8,128)(2,1)}, u32[]{:S(2)}) copy-start(bf16[16,1,512,256]{3,2,1,0:T(8,128)(2,1)} %param.22) | copy-start | bytes 12582916
  16.9 3.7 %copy-start.11 = (f32[128]{0:T(128)S(1)}, f32[128]{0:T(128)}, u32[]{:S(2)}) copy-start(f32[128]{0:T(128)} %param.28) | copy-start | bytes 1540
  19.6 15.0 %copy-start.6 = (f32[2048]{0:T(1024)S(1)}, f32[2048]{0:T(1024)}, u32[]{:S(2)}) copy-start(f32[2048]{0:T(1024)} %param.39) | copy-start | bytes 24580
  19.6 15.0 %copy-start.7 = (f32[2048]{0:T(1024)S(1)}, f32[2048]{0:T(1024)}, u32[]{:S(2)}) copy-start(f32[2048]{0:T(1024)} %param.30) | copy-start | bytes 24580
  19.6 17.0 %copy-start.8 = (s32[16,2]{0,1:T(2,128)S(1)}, s32[16,2]{0,1:T(2,128)}, u32[]{:S(2)}) copy-start(s32[16,2]{0,1:T(2,128)} %param.31) | copy-start | bytes 388
  20.0 57.4 %copy-start.12 = (u32[32]{0:T(128)S(1)}, u32[32]{0:T(128)}, u32[]{:S(2)}) copy-start(u32[32]{0:T(128)} %constant.87) | copy-start | bytes 388
  26.9 60.6 %copy-start.3 = (bf16[1,128,2048]{2,1,0:T(8,128)(2,1)S(1)}, bf16[1,128,2048]{2,1,0:T(8,128)(2,1)}, u32[]{:S(2)}) copy-start(bf16[1,128,2048]{2,1,0:T(8,128)(2,1)} %param.35) | copy-start | bytes 1572868
  34.9 6.5 %collective-permute-start = (bf16[4,2048]{1,0:T(4,128)(2,1)S(1)}, bf16[4,2048]{1,0:T(4,128)(2,1)S(1)}, u32[]{:S(2)}, u32[]{:S(2)}) collective-permute-start(bf16[4,2048]{1,0:T(4,128)(2,1)S(1)} %constant_dynamic-slice_fusion), channel_id=1, source_target_pairs={{0,4},{4,8},{8,12},{12,16},{16,20},{20,24},{24,28},{28,0},{1,5},{5... | collective-permute-start | bytes 49160 | tf_op jit(solution)/shard_map/ppermute | solution.py:193
  41.4 6.4 %collective-permute-start.1 = (bf16[4,2048]{1,0:T(4,128)(2,1)S(1)}, bf16[4,2048]{1,0:T(4,128)(2,1)S(1)}, u32[]{:S(2)}, u32[]{:S(2)}) collective-permute-start(bf16[4,2048]{1,0:T(4,128)(2,1)S(1)} %collective-permute-done), channel_id=1, source_target_pairs={{0,4},{4,8},{8,12},{12,16},{16,20},{20,24},{24,28},{28,0},{1,5},{5... | collective-permute-start | bytes 49160 | tf_op jit(solution)/shard_map/ppermute | solution.py:193
  47.8 6.4 %collective-permute-start.2 = (bf16[4,2048]{1,0:T(4,128)(2,1)S(1)}, bf16[4,2048]{1,0:T(4,128)(2,1)S(1)}, u32[]{:S(2)}, u32[]{:S(2)}) collective-permute-start(bf16[4,2048]{1,0:T(4,128)(2,1)S(1)} %collective-permute-done.1), channel_id=1, source_target_pairs={{0,4},{4,8},{8,12},{12,16},{16,20},{20,24},{24,28},{28,0},{1,5},{5... | collective-permute-start | bytes 49160 | tf_op jit(solution)/shard_map/ppermute | solution.py:193
  54.2 6.4 %collective-permute-start.3 = (bf16[4,2048]{1,0:T(4,128)(2,1)S(1)}, bf16[4,2048]{1,0:T(4,128)(2,1)S(1)}, u32[]{:S(2)}, u32[]{:S(2)}) collective-permute-start(bf16[4,2048]{1,0:T(4,128)(2,1)S(1)} %collective-permute-done.2), channel_id=1, source_target_pairs={{0,4},{4,8},{8,12},{12,16},{16,20},{20,24},{24,28},{28,0},{1,5},{5... | collective-permute-start | bytes 49160 | tf_op jit(solution)/shard_map/ppermute | solution.py:193
  60.7 7.0 %collective-permute-start.4 = (bf16[4,2048]{1,0:T(4,128)(2,1)S(1)}, bf16[4,2048]{1,0:T(4,128)(2,1)S(1)}, u32[]{:S(2)}, u32[]{:S(2)}) collective-permute-start(bf16[4,2048]{1,0:T(4,128)(2,1)S(1)} %collective-permute-done.3), channel_id=1, source_target_pairs={{0,4},{4,8},{8,12},{12,16},{16,20},{20,24},{24,28},{28,0},{1,5},{5... | collective-permute-start | bytes 49160 | tf_op jit(solution)/shard_map/ppermute | solution.py:193
  61.6 24.6 %all-to-all-start = ((bf16[8,8,2048]{2,1,0:T(8,128)(2,1)}), bf16[8,8,2048]{2,1,0:T(8,128)(2,1)S(1)}, u32[]{:S(2)}, u32[]{:S(2)}) async-start(bf16[8,8,2048]{2,1,0:T(8,128)(2,1)} %fusion), calls=%async_computation | async-start | bytes 524288 | tf_op jit(solution)/shard_map/all_to_all | solution.py:169
  67.6 71.1 %reduce-scatter.2.cloned.1.call-start = ((), (), s32[]{:S(2)}) async-start(), calls=%async_computation.4 | async-start | bytes 327680 | tf_op jit(solution)/shard_map/reduce_scatter | solution.py:179
  67.7 8.9 %collective-permute-start.5 = (bf16[4,2048]{1,0:T(4,128)(2,1)S(1)}, bf16[4,2048]{1,0:T(4,128)(2,1)S(1)}, u32[]{:S(2)}, u32[]{:S(2)}) collective-permute-start(bf16[4,2048]{1,0:T(4,128)(2,1)S(1)} %collective-permute-done.4), channel_id=1, source_target_pairs={{0,4},{4,8},{8,12},{12,16},{16,20},{20,24},{24,28},{28,0},{1,5},{5... | collective-permute-start | bytes 49160 | tf_op jit(solution)/shard_map/ppermute | solution.py:193
  76.5 6.4 %collective-permute-start.6 = (bf16[4,2048]{1,0:T(4,128)(2,1)S(1)}, bf16[4,2048]{1,0:T(4,128)(2,1)S(1)}, u32[]{:S(2)}, u32[]{:S(2)}) collective-permute-start(bf16[4,2048]{1,0:T(4,128)(2,1)S(1)} %collective-permute-done.5), channel_id=1, source_target_pairs={{0,4},{4,8},{8,12},{12,16},{16,20},{20,24},{24,28},{28,0},{1,5},{5... | collective-permute-start | bytes 49160 | tf_op jit(solution)/shard_map/ppermute | solution.py:193
  89.7 45.2 %copy-start.9 = (f32[16,2]{0,1:T(2,128)S(1)}, f32[16,2]{0,1:T(2,128)}, u32[]{:S(2)}) copy-start(f32[16,2]{0,1:T(2,128)} %param.32) | copy-start | bytes 388
  131.6 7.1 %all-to-all-start.2 = ((bf16[4,4,512]{2,0,1:T(4,128)(2,1)}), bf16[4,4,512]{2,0,1:T(4,128)(2,1)S(1)}, u32[]{:S(2)}, u32[]{:S(2)}) async-start(bf16[4,4,512]{2,0,1:T(4,128)(2,1)} %bitcast.34), calls=%async_computation.3 | async-start | bytes 32768 | tf_op jit(solution)/shard_map/all_to_all | solution.py:206
  138.7 10.7 %all-to-all-start.1 = ((bf16[8,8,512]{2,1,0:T(8,128)(2,1)}), bf16[8,8,512]{2,1,0:T(8,128)(2,1)S(1)}, u32[]{:S(2)}, u32[]{:S(2)}) async-start(bf16[8,8,512]{2,1,0:T(8,128)(2,1)} %reduce-scatter.2.cloned.1.call-done), calls=%async_computation.2 | async-start | bytes 131072 | tf_op jit(solution)/shard_map/all_to_all | solution.py:182
Sparse Core Ops, SparseCore 0:
  89.8 17.5 reduce-scatter.1
